TPU v7x, 32 devices: a whole 2x2x4 slice. The times are simulated.
32 devices in a mesh: fs: 16 (over z, y, x), tp: 2 (over core).
Axes of the slice: x: 2, y: 2, z: 4, core: 2. Of those that a mesh axis runs over, the one named last changes fastest.
Arguments:
- saved_input: bfloat16 [16384, 2048], P('fs'), may hold values from -60 to 60
- out_cotangent: bfloat16 [16384, 4096], P('fs', 'tp'), may hold values from -6 to 6
- old_weight: float32 [2048, 4096], P('fs', 'tp'), may hold values from -0.125 to 0.125
- factor: bfloat16 [4096, 256], P('tp'), may hold values from -0.09375 to 0.09375
- moment_first: float32 [2048, 256], P('fs'), may hold values from -3 to 3
- moment_second: float32 [2048, 256], P('fs'), may hold values from 0.05 to 1
Outputs:
- new_weight: float32 [2048, 4096], P('fs', 'tp')
- update: float32 [2048, 4096], P('fs', 'tp')
- new_first: float32 [2048, 256], P('fs')
- new_second: float32 [2048, 256], P('fs')
- weight_copy: bfloat16 [2048, 4096], P(None, 'tp')
All inputs are finite; a program needn't handle non-finite values.
Results may differ from a plain program's by a relative error of at most 0.0028.
Values may be sent and summed in bfloat16 or wider, within the bound.
A program may use at most 64 MiB of HBM per device.

v0:
```python
import math

import jax
import jax.numpy as jnp
from jax import lax
from jax.sharding import PartitionSpec as P

HV = 2048
RANK = 256


def on_device(saved_input, out_cotangent, old_weight, factor, moment_first, moment_second):
    wide_factor = factor.astype(jnp.float32)
    contract = (((0,), (0,)), ((), ()))
    reduced = jnp.dot(out_cotangent, factor, preferred_element_type=jnp.float32)
    reduced_high = reduced.astype(jnp.bfloat16)
    reduced_low = (reduced - reduced_high.astype(jnp.float32)).astype(jnp.bfloat16)
    high_part = lax.dot_general(
        saved_input, reduced_high, contract, preferred_element_type=jnp.float32
    )
    low_part = lax.dot_general(
        saved_input, reduced_low, contract, preferred_element_type=jnp.float32
    )
    shard = lax.psum_scatter(high_part + low_part, ("fs", "tp"), scatter_dimension=0, tiled=True)
    projected = lax.all_gather(shard, "tp", axis=0, tiled=True)
    squares = lax.psum(jnp.sum(projected * projected), "fs")
    clip = jnp.minimum(1.0, math.sqrt(HV * RANK) / (jnp.sqrt(squares) + 1e-06))
    clipped = clip * projected
    new_first = 0.9 * moment_first + 0.1 * clipped
    new_second = 0.95 * moment_second + 0.05 * clipped * clipped
    direction = new_first / (jnp.sqrt(new_second) + 1e-08)
    update = jnp.dot(direction, wide_factor.T, precision=lax.Precision.HIGHEST)
    new_weight = old_weight - 0.05 * update
    copied = lax.all_gather(new_weight.astype(jnp.bfloat16), "fs", axis=0, tiled=True)
    return (new_weight, update, new_first, new_second, copied)


def solution(mesh):
    return jax.shard_map(
        on_device,
        mesh=mesh,
        in_specs=(
            P("fs", None),
            P("fs", "tp"),
            P("fs", "tp"),
            P("tp", None),
            P("fs", None),
            P("fs", None),
        ),
        out_specs=(P("fs", "tp"), P("fs", "tp"), P("fs", None), P("fs", None), P(None, "tp")),
        check_vma=False,
    )
```

profile of v0, /device:TPU:0, one launch (start us, length us, event | category | flops | bytes accessed | tf_op | source)
XLA Modules:
  0.0 327.6 jit_solution(6822291514457677202)
XLA Ops:
  7.2 0.0 copy-start
  7.2 0.0 reduce-scatter.4.cloned.1.call-start
  7.2 1.2 copy-done
  8.4 0.0 copy-start.1
  8.4 3.6 %fusion.12 = f32[1024,256]{1,0:T(8,128)S(1)} fusion(bf16[1024,2048]{1,0:T(8,128)(2,1)} %param.7, bf16[2048,256]{1,0:T(8,128)(2,1)S(1)} %copy-done), kind=kOutput, calls=%fused_computation.18 | convolution fusion | flops 1073741824 | bytes 6291456 | tf_op jit(solution)/shard_map/dot_general | solution.py:15
  12.0 0.0 copy-done.1
  12.0 1.3 fusion.2
  13.3 1.3 fusion
  14.6 0.0 copy-start.4
  14.6 0.0 copy-start.5
  14.6 1.8 copy.16
  16.4 0.0 reduce-scatter.4.cloned.1.call-update
  16.4 0.0 all-gather.2.cloned.1.call-start
  16.5 140.9 %reduce-scatter.4.cloned.1.call-done = f32[64,256]{1,0:T(8,128)} async-done(((f32[2048,256]{1,0:T(8,128)}), f32[64,256]{1,0:T(8,128)}) %reduce-scatter.4.cloned.1.call-update) | async-done | bytes 65552 | tf_op jit(solution)/shard_map/reduce_scatter | solution.py:24
  157.4 2.1 all_gather.6
  159.5 0.6 multiply_reduce_fusion
  160.1 37.3 %psum.7 = f32[]{:T(128)} all-reduce(f32[]{:T(128)} %multiply_reduce_fusion), channel_id=1, replica_groups=mesh['fs'=16,'tp'=2] {'fs'}, use_global_device_ids=true, to_apply=%region_2.0 | all-reduce | flops 1 | bytes 8 | tf_op jit(solution)/shard_map/psum | solution.py:26
  198.1 0.0 copy-done.4
  198.1 0.0 copy-done.5
  198.2 0.0 copy-start.2
  198.2 0.0 copy-start.3
  198.2 4.0 %fusion.11 = (bf16[128,2048]{1,0:T(8,128)(2,1)}, f32[128,2048]{1,0:T(8,128)}, f32[128,2048]{1,0:T(8,128)}) fusion(f32[128,2048]{1,0:T(8,128)} %param.8, bf16[2048,256]{1,0:T(8,128)(2,1)S(1)} %copy-done, f32[128,256]{1,0:T(8,128)S(1)} %get-tuple-element.22, f32[128,256]{1,0:T(8,128)S(1)} %get-tuple-element.23), kind=kOutput, calls=%fused_computation.17 | convolution fusion | flops 806158336 | bytes 4980736 | tf_op jit(solution)/shard_map/dot_general | solution.py:32
  202.2 0.0 all-gather.2.cloned.1.call-update
  202.2 110.1 %all-gather.2.cloned.1.call-done = bf16[2048,2048]{1,0:T(8,128)(2,1)} async-done(((bf16[128,2048]{1,0:T(8,128)(2,1)}), bf16[2048,2048]{1,0:T(8,128)(2,1)}) %all-gather.2.cloned.1.call-update) | async-done | bytes 8388624 | tf_op jit(solution)/shard_map/all_gather | solution.py:34
  312.3 8.4 %copy.19 = bf16[2048,2048]{1,0:T(8,128)(2,1)} copy(bf16[2048,2048]{1,0:T(8,128)(2,1)} %all-gather.2.cloned.1.call-done) | data formatting | bytes 16777216
  320.8 0.0 copy-done.2
  320.8 0.0 copy-done.3
  (1 shorter events, 0.0 us)
Async XLA Ops:
  7.2 1.2 copy-start
  7.2 150.2 %reduce-scatter.4.cloned.1.call-start = ((), (), s32[]{:S(2)}) async-start(), calls=%async_computation.2 | async-start | bytes 2162688 | tf_op jit(solution)/shard_map/reduce_scatter | solution.py:24
  8.4 3.6 %copy-start.1 = (bf16[1024,2048]{1,0:T(8,128)(2,1)S(1)}, bf16[1024,2048]{1,0:T(8,128)(2,1)}, u32[]{:S(2)}) copy-start(bf16[1024,2048]{1,0:T(8,128)(2,1)} %param.6) | copy-start | bytes 12582916
  14.6 183.6 %copy-start.4 = (f32[128,256]{1,0:T(8,128)S(1)}, f32[128,256]{1,0:T(8,128)}, u32[]{:S(2)}) copy-start(f32[128,256]{1,0:T(8,128)} %param.11) | copy-start | bytes 393220
  14.6 183.6 %copy-start.5 = (f32[128,256]{1,0:T(8,128)S(1)}, f32[128,256]{1,0:T(8,128)}, u32[]{:S(2)}) copy-start(f32[128,256]{1,0:T(8,128)} %param.10) | copy-start | bytes 393220
  16.4 295.9 %all-gather.2.cloned.1.call-start = ((), (), s32[]{:S(2)}) async-start(), calls=%async_computation.1 | async-start | bytes 8912896 | tf_op jit(solution)/shard_map/all_gather | solution.py:34
  198.2 122.6 %copy-start.2 = (f32[128,256]{1,0:T(8,128)}, f32[128,256]{1,0:T(8,128)S(1)}, u32[]{:S(2)}) copy-start(f32[128,256]{1,0:T(8,128)S(1)} %get-tuple-element.23) | copy-start | bytes 393220
  198.2 122.6 %copy-start.3 = (f32[128,256]{1,0:T(8,128)}, f32[128,256]{1,0:T(8,128)S(1)}, u32[]{:S(2)}) copy-start(f32[128,256]{1,0:T(8,128)S(1)} %get-tuple-element.22) | copy-start | bytes 393220
Sparse Core Ops, SparseCore 0:
  16.5 140.7 reduce-scatter.3
  202.3 109.9 all-gather.1
where the time goes:
time: 328 us
  waiting for transfers between devices  251 us (77%)
  blocking collectives  39.4 us (12%)
  between operations  14.9 us (5%)
  local copies, waits for them, and re-layouts  11.5 us (4%)
  matrix products  10.1 us (3%)
    reduce_scatter x1, waiting for transfers between devices, on_device(): lax.psum_scatter(high_part + low_part, ('fs', 'tp'), scatter_dimension=0,...  141 us
    all_gather x1, waiting for transfers between devices, on_device(): lax.all_gather(new_weight.astype(jnp.bfloat16), 'fs', axis=0, tiled=True)  110 us
    psum x1, blocking collectives, on_device(): squares = lax.psum(jnp.sum(projected * projected), 'fs')  37.3 us
    unnamed x14, local copies, waits for them, and re-layouts  11.5 us
  transfers between devices with their start and end apart: 2, of which 2 were waited for; matrix products, arithmetic and copies ran while one was open for 0% of the time, Pallas kernels for 0%

commit v1 on v0

v1 whole, which is shorter than its diff:
```python
import functools
import math

import jax
import jax.numpy as jnp
from jax import lax
from jax.experimental import pallas as pl
from jax.experimental.pallas import tpu as pltpu
from jax.sharding import PartitionSpec as P

F32, BF16 = jnp.float32, jnp.bfloat16
MESH = pl.DeviceIdType.MESH
LIMIT = 0.125
SPAN = 120.0
SLOPE = 2 * SPAN / LIMIT


def encode(weight):
    size = jnp.exp2(jnp.abs(weight) * SLOPE - SPAN)
    return jnp.where(weight < 0, -size, size).astype(BF16)


def decode(code):
    code = code.astype(F32)
    size = jnp.log2(jnp.abs(code)) * (1 / SLOPE) + SPAN / SLOPE
    return jnp.where(code < 0, -size, size)


def plain(saved_input, out_cotangent, old_weight, factor, moment_first, moment_second):
    wide_factor = factor.astype(F32)
    contract = (((0,), (0,)), ((), ()))
    reduced = jnp.dot(out_cotangent, factor, preferred_element_type=F32)
    high = reduced.astype(BF16)
    low = (reduced - high.astype(F32)).astype(BF16)
    high_part = lax.dot_general(saved_input, high, contract, preferred_element_type=F32)
    low_part = lax.dot_general(saved_input, low, contract, preferred_element_type=F32)
    shard = lax.psum_scatter(high_part + low_part, ("fs", "tp"), scatter_dimension=0, tiled=True)
    projected = lax.all_gather(shard, "tp", axis=0, tiled=True)
    squares = lax.psum(jnp.sum(projected * projected), "fs")
    entries = saved_input.shape[1] * factor.shape[1]
    clip = jnp.minimum(1.0, math.sqrt(entries) / (jnp.sqrt(squares) + 1e-06))
    clipped = clip * projected
    new_first = 0.9 * moment_first + 0.1 * clipped
    new_second = 0.95 * moment_second + 0.05 * clipped * clipped
    direction = new_first / (jnp.sqrt(new_second) + 1e-08)
    update = jnp.dot(direction, wide_factor.T, precision=lax.Precision.HIGHEST)
    new_weight = old_weight - 0.05 * update
    copied = lax.all_gather(new_weight.astype(BF16), "fs", axis=0, tiled=True)
    return (new_weight, update, new_first, new_second, copied)


def exchange(n, entries, old, saved_hbm, cot_hbm, fac_hbm, m1, m2,
             gath, dirbuf, dirf, nf, ns,
             old16, saved, cot, fac, ybuf, pbuf, xbuf, sbuf, rbuf, projv, sqbuf,
             in_sem, own_sem, send_sem, recv_sem, pair_sem,
             ps_sem, pr_sem, qs_sem, qr_sem, ds_sem, dr_sem):
    me, c = lax.axis_index("fs"), lax.axis_index("tp")
    nz = n // 4
    x, y, z = lax.rem(me, 2), lax.rem(me // 2, 2), me // 4
    xn = me + 1 - 2 * x
    yn = me + 2 - 4 * y
    xyn = xn + 2 - 4 * y
    has_up, has_dn = z + 1 < nz, z > 0
    unit = old.shape[0] // 8
    parts = [(0, 3 * unit), (3 * unit, 3 * unit), (6 * unit, unit), (7 * unit, unit)]
    half = old.shape[0] // 2
    contract = (((0,), (0,)), ((), ()))

    loads = [pltpu.make_async_copy(a, b, in_sem.at[i])
             for i, (a, b) in enumerate([(cot_hbm, cot), (fac_hbm, fac), (saved_hbm, saved)])]
    for load in loads:
        load.start()
    barrier = pltpu.get_barrier_semaphore()

    def greet(k, _):
        pl.semaphore_signal(barrier, inc=1, device_id=(lax.rem(me + k, n), c), device_id_type=MESH)
        return 0

    lax.fori_loop(1, n, greet, 0)
    pl.semaphore_signal(barrier, inc=1, device_id=(me, 1 - c), device_id_type=MESH)
    piece = old.shape[0] // 4
    for k in range(4):
        old16[pl.ds(k * piece, piece)] = encode(old[pl.ds(k * piece, piece)])
    own_copy = pltpu.make_async_copy(old16, gath.at[me], own_sem)
    own_copy.start()
    pl.semaphore_wait(barrier, n)

    pending = []

    def send(cls, origin, target, own=False, cond=None):
        site = len(pending)
        first, count = parts[cls]

        def make():
            src = old16.at[pl.ds(first, count)] if own else gath.at[origin, pl.ds(first, count)]
            return pltpu.make_async_remote_copy(
                src, gath.at[origin, pl.ds(first, count)], send_sem.at[site],
                recv_sem.at[cls, origin], device_id=(target, c), device_id_type=MESH)

        pending.append((make, cond))
        if cond is None:
            make().start()
        else:
            @pl.when(cond)
            def _():
                make().start()

    def recv(cls, origin, cond=None):
        first, count = parts[cls]

        def wait():
            piece = gath.at[origin, pl.ds(first, count)]
            pltpu.make_async_remote_copy(
                piece, piece, send_sem.at[0], recv_sem.at[cls, origin],
                device_id=(me, c), device_id_type=MESH).wait_recv()

        if cond is None:
            wait()
        else:
            pl.when(cond)(wait)

    up, dn = me + 4, me - 4

    for cls, order in ((2, (xn, yn)), (3, (yn, xn))):
        for target in order:
            send(cls, me, target, own=True)
    for cls, order in ((0, (xn, yn)), (1, (yn, xn))):
        send(cls, me, up, own=True, cond=has_up)
        send(cls, me, dn, own=True, cond=has_dn)
        for target in order:
            send(cls, me, target, own=True)
    for cls in (2, 3):
        send(cls, me, up, own=True, cond=has_up)
        send(cls, me, dn, own=True, cond=has_dn)

    def sides(s):
        yield -4 * s, z >= s, up, has_up
        yield 4 * s, z + s < nz, dn, has_dn

    def a_line(cls, s):
        near = (xn, yn) if cls == 0 else (yn, xn)
        for shift, there, ahead, more in sides(s):
            recv(cls, me + shift, there)
            if s + 1 < nz:
                send(cls, me + shift, ahead, cond=jnp.logical_and(there, more))
            for target in near:
                send(cls, me + shift, target, cond=there)

    def a_cross(cls, s):
        near, far = (xn, yn) if cls == 0 else (yn, xn)
        if s == 0:
            recv(cls, near)
            send(cls, near, far)
            return
        for shift, there, _, _ in sides(s):
            recv(cls, near + shift, there)
            send(cls, near + shift, far, cond=there)

    def a_last(cls, s):
        near, far = (xn, yn) if cls == 0 else (yn, xn)
        for origin in (far, xyn):
            if s == 0:
                recv(cls, origin)
                continue
            for shift, there, _, _ in sides(s):
                recv(cls, origin + shift, there)

    def c_flat(cls, origin, forward=None):
        recv(cls, origin)
        if forward is not None:
            send(cls, origin, forward)
        send(cls, origin, up, cond=has_up)
        send(cls, origin, dn, cond=has_dn)

    def c_line(cls, s):
        for origin in (me, xn, yn, xyn) if cls == 2 else (me, yn, xn, xyn):
            for shift, there, ahead, more in sides(s):
                recv(cls, origin + shift, there)
                if s + 1 < nz:
                    send(cls, origin + shift, ahead, cond=jnp.logical_and(there, more))

    loads[0].wait()
    loads[1].wait()
    tall = cot.shape[0] // 4

    def reduce_rows(k, _):
        rows = pl.ds(pl.multiple_of(k * tall, tall), tall)
        value = jnp.dot(cot[rows, :], fac[...], preferred_element_type=F32)
        high = value.astype(BF16)
        ybuf[0, rows, :] = high
        ybuf[1, rows, :] = (value - high.astype(F32)).astype(BF16)
        return 0

    lax.fori_loop(0, 4, reduce_rows, 0)
    loads[2].wait()
    wide = 4 * half

    def project(k, _):
        cols = saved[:, pl.ds(pl.multiple_of(k * wide, wide), wide)]
        value = lax.dot_general(cols, ybuf[0], contract, preferred_element_type=F32)
        value = value + lax.dot_general(cols, ybuf[1], contract, preferred_element_type=F32)
        pbuf[pl.ds(2 * k, 2)] = value.reshape((2, 2, half, value.shape[1]))
        return 0

    lax.fori_loop(0, n // 2, project, 0)

    def pair_copy(i, src, dst):
        return pltpu.make_async_remote_copy(
            src, dst, pair_sem.at[2 * i], pair_sem.at[2 * i + 1],
            device_id=(me, 1 - c), device_id_type=MESH)

    swap = pair_copy(0, pbuf.at[:, 1 - c], xbuf)
    swap.start()

    a_line(0, 1)
    a_line(1, 1)
    c_flat(2, xn, yn)
    c_flat(3, yn, xn)

    swap.wait()

    def chip_sum(k, _):
        value = pbuf[k, c] + xbuf[k]
        xbuf[k] = value
        sbuf[k] = value.astype(BF16)
        return 0

    lax.fori_loop(0, n, chip_sum, 0)

    def to_owner(k):
        peer = lax.rem(me + k, n)
        return pltpu.make_async_remote_copy(
            sbuf.at[peer], rbuf.at[me], ps_sem.at[peer], pr_sem.at[me],
            device_id=(peer, c), device_id_type=MESH)

    def from_peer(k, buf, sem):
        peer = lax.rem(me + k, n)
        return pltpu.make_async_remote_copy(
            buf, buf, sem, sem, device_id=(me, c), device_id_type=MESH)

    def start_owner(k, _):
        to_owner(k).start()
        return 0

    lax.fori_loop(1, n, start_owner, 0)

    a_cross(0, 0)
    a_cross(1, 0)
    c_flat(2, yn)
    c_flat(3, xn)
    c_flat(2, xyn)
    c_flat(3, xyn)
    if nz > 2:
        a_line(0, 2)
        a_line(1, 2)
    a_cross(0, 1)
    a_cross(1, 1)

    def take(k, _):
        peer = lax.rem(me + k, n)
        from_peer(k, rbuf.at[peer], pr_sem.at[peer]).wait_recv()
        return 0

    lax.fori_loop(1, n, take, 0)

    def add(k, total):
        return total + rbuf[lax.rem(me + k, n)].astype(F32)

    projv[c] = lax.fori_loop(1, n, add, xbuf[me])
    share = pair_copy(1, projv.at[c], projv.at[c])
    share.start()
    c_line(2, 1)
    c_line(3, 1)
    share.wait()
    projected = projv[...]
    sqbuf[me] = jnp.full(sqbuf.shape[1:], jnp.sum(projected * projected), F32)

    def to_all(k):
        peer = lax.rem(me + k, n)
        return pltpu.make_async_remote_copy(
            sqbuf.at[me], sqbuf.at[me], qs_sem.at[peer], qr_sem.at[me],
            device_id=(peer, c), device_id_type=MESH)

    def start_all(k, _):
        to_all(k).start()
        return 0

    lax.fori_loop(1, n, start_all, 0)
    for s in range(3, nz):
        a_line(0, s)
        a_line(1, s)
    if nz > 2:
        a_cross(0, 2)
        a_cross(1, 2)
        c_line(2, 2)
        c_line(3, 2)

    def take_squares(k, _):
        peer = lax.rem(me + k, n)
        from_peer(k, sqbuf.at[peer], qr_sem.at[peer]).wait_recv()
        return 0

    lax.fori_loop(1, n, take_squares, 0)
    squares = sqbuf[0]
    for k in range(1, n):
        squares = squares + sqbuf[k]
    clip = jnp.minimum(1.0, math.sqrt(entries) / (jnp.sqrt(squares) + 1e-06))[0:1]
    for h in range(2):
        rows = pl.ds(h * half, half)
        clipped = clip * projv[h]
        first = 0.9 * m1[rows] + 0.1 * clipped
        second = 0.95 * m2[rows] + 0.05 * clipped * clipped
        nf[rows] = first
        ns[rows] = second
        dirf[rows] = first / (jnp.sqrt(second) + 1e-08)
    dirbuf[me, c] = dirf[pl.ds(pl.multiple_of(c * half, half), half)].astype(BF16)

    def direction_to(k):
        peer = lax.rem(me + k, n)
        return pltpu.make_async_remote_copy(
            dirbuf.at[me, c], dirbuf.at[me, c], ds_sem.at[peer], dr_sem.at[me],
            device_id=(peer, c), device_id_type=MESH)

    def start_direction(k, _):
        direction_to(k).start()
        return 0

    lax.fori_loop(1, n, start_direction, 0)
    for s in range(3, nz):
        a_cross(0, s)
        a_cross(1, s)
        c_line(2, s)
        c_line(3, s)

    def take_direction(k, _):
        peer = lax.rem(me + k, n)
        from_peer(k, dirbuf.at[peer, c], dr_sem.at[peer]).wait_recv()
        return 0

    lax.fori_loop(1, n, take_direction, 0)
    halves = pair_copy(2, dirbuf.at[:, c], dirbuf.at[:, c])
    halves.start()
    for s in range(nz):
        a_last(0, s)
        a_last(1, s)
    halves.wait()
    own_copy.wait()

    def finish(k, _):
        to_owner(k).wait_send()
        to_all(k).wait_send()
        direction_to(k).wait_send()
        return 0

    lax.fori_loop(1, n, finish, 0)
    for make, cond in pending:
        if cond is None:
            make().wait_send()
        else:
            @pl.when(cond)
            def _(make=make):
                make().wait_send()


def sites(nz):
    flat = 16 + 2 * 7
    line = sum((2 * 2 * 3 if s + 1 < nz else 2 * 2 * 2) for s in range(1, nz))
    cross = 2 * (1 + 2 * (nz - 1))
    columns = sum(2 * 4 * 2 for s in range(1, nz) if s + 1 < nz)
    return flat + line + cross + columns


def overlapped(n, saved_input, out_cotangent, old_weight, factor, moment_first, moment_second):
    rows, width = old_weight.shape
    rank = factor.shape[1]
    half = rows // 2
    entries = saved_input.shape[1] * rank
    any_space = pl.BlockSpec(memory_space=pl.ANY)
    vmem = pl.BlockSpec(memory_space=pltpu.VMEM)
    shape = jax.ShapeDtypeStruct
    sem = pltpu.SemaphoreType.DMA
    gath, dirbuf, direction, new_first, new_second = pl.pallas_call(
        functools.partial(exchange, n, entries),
        out_shape=[
            shape((n, rows, width), BF16),
            shape((n, 2, half, rank), BF16),
            shape((rows, rank), F32),
            shape((rows, rank), F32),
            shape((rows, rank), F32),
        ],
        in_specs=[vmem, any_space, any_space, any_space, vmem, vmem],
        out_specs=[any_space, vmem, vmem, vmem, vmem],
        scratch_shapes=[
            pltpu.VMEM((rows, width), BF16),
            pltpu.VMEM(saved_input.shape, BF16),
            pltpu.VMEM(out_cotangent.shape, BF16),
            pltpu.VMEM(factor.shape, BF16),
            pltpu.VMEM((2, saved_input.shape[0], rank), BF16),
            pltpu.VMEM((n, 2, half, rank), F32),
            pltpu.VMEM((n, half, rank), F32),
            pltpu.VMEM((n, half, rank), BF16),
            pltpu.VMEM((n, half, rank), BF16),
            pltpu.VMEM((2, half, rank), F32),
            pltpu.VMEM((n, 8, rank), F32),
            sem((3,)), sem, sem((sites(n // 4),)), sem((4, n)), sem((6,)),
            sem((n,)), sem((n,)), sem((n,)), sem((n,)), sem((n,)), sem((n,)),
        ],
        compiler_params=pltpu.CompilerParams(
            collective_id=0, has_side_effects=True, vmem_limit_bytes=48 * 2**20
        ),
    )(old_weight, saved_input, out_cotangent, factor, moment_first, moment_second)
    across = (((1,), (1,)), ((), ()))
    every = lax.dot_general(
        dirbuf.reshape((n * rows, rank)), factor, across, preferred_element_type=F32
    )
    copied = (decode(gath.reshape((n * rows, width))) - 0.05 * every).astype(BF16)
    update = lax.dot_general(
        direction, factor.astype(F32), across, precision=lax.Precision.HIGHEST
    )
    new_weight = old_weight - 0.05 * update
    return (new_weight, update, new_first, new_second, copied)


def solution(mesh):
    n, pair = mesh.shape["fs"], mesh.shape["tp"]

    def on_device(*args):
        rows = args[2].shape[0]
        if pair == 2 and n % 4 == 0 and n >= 8 and rows % 128 == 0:
            return overlapped(n, *args)
        return plain(*args)

    return jax.shard_map(
        on_device,
        mesh=mesh,
        in_specs=(
            P("fs", None),
            P("fs", "tp"),
            P("fs", "tp"),
            P("tp", None),
            P("fs", None),
            P("fs", None),
        ),
        out_specs=(P("fs", "tp"), P("fs", "tp"), P("fs", None), P("fs", None), P(None, "tp")),
        check_vma=False,
    )
```

time: 328 us -> 131 us (0.40)
  waiting for transfers between devices: 251 us -> 0 us
  Pallas kernels: 0 us -> 89.9 us
  blocking collectives: 39.4 us -> 0 us
  other arithmetic: 0.67 us -> 21.3 us
  between operations: 14.9 us -> 0.66 us
  local copies, waits for them, and re-layouts: 11.5 us -> 5.57 us
  matrix products: 10.1 us -> 13.6 us
    reduce_scatter x1 -> x0, waiting for transfers between devices: 141 us -> none  [on_device(): lax.psum_scatter(high_part + low_part, ('fs', 'tp'), scatter_dimension=0,...]
    all_gather x1 -> x0, waiting for transfers between devices: 110 us -> none  [on_device(): lax.all_gather(new_weight.astype(jnp.bfloat16), 'fs', axis=0, tiled=True)]
    pallas_call x0 -> x1, Pallas kernels: none -> 89.9 us  [overlapped(): pl.pallas_call(functools.partial(exchange, n, entries), out_shape=[shape(...]
    psum x1 -> x0, blocking collectives: 37.3 us -> none  [on_device(): squares = lax.psum(jnp.sum(projected * projected), 'fs')]
    add x1, other arithmetic: 0.04 us -> 13.2 us  [decode(): size = jnp.log2(jnp.abs(code)) * (1 / SLOPE) + SPAN / SLOPE]
    lt x0 -> x1, other arithmetic: none -> 8.1 us  [decode(): return jnp.where(code < 0, -size, size)]
    unnamed x14, local copies, waits for them, and re-layouts: 11.5 us -> 5.57 us
    dot_general x4 -> x2, matrix products: 10.1 us -> 13.6 us  [the longest x1 11.1 us: overlapped(): lax.dot_general(dirbuf.reshape((n * rows, rank)), factor, across, preferr...]
  transfers between devices with their start and end apart: 2 -> 0, of which waited for: 2 -> 0; matrix products, arithmetic and copies ran while one was open for 0% -> 0% of each run, Pallas kernels for 0% -> 0%
where the time goes in v1:
time: 131 us
  Pallas kernels  89.9 us (69%)
  other arithmetic  21.3 us (16%)
  matrix products  13.6 us (10%)
  local copies, waits for them, and re-layouts  5.57 us (4%)
    pallas_call x1, Pallas kernels, overlapped(): pl.pallas_call(functools.partial(exchange, n, entries), out_shape=[shape(...  89.9 us
    add x1, other arithmetic, decode(): size = jnp.log2(jnp.abs(code)) * (1 / SLOPE) + SPAN / SLOPE  13.2 us
    dot_general x1, matrix products, overlapped(): lax.dot_general(dirbuf.reshape((n * rows, rank)), factor, across, preferr...  11.1 us
    lt x1, other arithmetic, decode(): return jnp.where(code < 0, -size, size)  8.1 us
    unnamed x14, local copies, waits for them, and re-layouts  5.57 us

profile of v1, /device:TPU:0, one launch (start us, length us, event | category | flops | bytes accessed | tf_op | source)
XLA Modules:
  0.0 131.0 jit_solution(4450321464306923510)
XLA Ops:
  0.6 0.0 copy-start
  0.6 1.2 copy-done
  1.9 0.0 copy-start.2
  1.9 1.2 copy-done.2
  3.1 0.0 copy-start.4
  3.1 0.9 copy-done.4
  4.0 0.0 copy-start.5
  4.0 0.9 copy-done.5
  4.9 89.9 %shard_map.101 = (bf16[16,128,2048]{2,1,0:T(8,128)(2,1)}, bf16[16,2,64,256]{3,2,1,0:T(8,128)(2,1)S(1)}, f32[128,256]{1,0:T(8,128)S(1)}, f32[128,256]{1,0:T(8,128)S(1)}, f32[128,256]{1,0:T(8,128)S(1)}) custom-call(f32[128,2048]{1,0:T(8,128)S(1)} %copy-done.2, bf16[1024,2048]{1,0:T(8,128)(2,1)} %saved_hbm.1, bf16[1024,2048]{1,0:T(8,128)(2,1)} %cot_hbm.1, ...), custom_call_target="tpu_custom_call" | custom-call | tf_op jit(solution)/shard_map/pallas_call | solution.py:382
  94.8 0.0 copy-start.1
  94.8 13.2 %fusion.2 = f32[16,128,2048]{2,1,0:T(8,128)} fusion(bf16[16,128,2048]{2,1,0:T(8,128)(2,1)} %get-tuple-element.13), kind=kLoop, calls=%fused_computation.5 | loop fusion | flops 16777216 | bytes 25165824 | tf_op jit(solution)/shard_map/add | solution.py:25
  108.0 8.1 %convert_compare_fusion = pred[16,128,2048]{2,1,0:T(32,128)(4,1)} fusion(bf16[16,128,2048]{2,1,0:T(8,128)(2,1)} %get-tuple-element.13), kind=kLoop, calls=%fused_computation.2 | loop fusion | flops 8388608 | bytes 12582912 | tf_op jit(solution)/shard_map/lt | solution.py:26
  116.1 0.0 copy-start.3
  116.1 0.0 copy-done.1
  116.1 11.1 %fusion.4 = bf16[2048,2048]{1,0:T(8,128)(2,1)} fusion(f32[16,128,2048]{2,1,0:T(8,128)} %fusion.2, pred[16,128,2048]{2,1,0:T(32,128)(4,1)} %convert_compare_fusion, bf16[2048,256]{1,0:T(8,128)(2,1)S(1)} %bitcast.9, bf16[2048,256]{1,0:T(8,128)(2,1)S(1)} %copy-done.1), kind=kOutput, calls=%fused_computation.7 | convolution fusion | flops 2168455168 | bytes 31457280 | tf_op jit(solution)/shard_map/dot_general | solution.py:413
  127.2 0.0 copy-done.3
  127.2 2.5 %multiply_subtract_fusion = (f32[128,2048]{1,0:T(8,128)}, f32[128,2048]{1,0:T(8,128)}) fusion(f32[128,2048]{1,0:T(8,128)S(1)} %copy-done.3, f32[128,256]{1,0:T(8,128)S(1)} %get-tuple-element.10, bf16[2048,256]{1,0:T(8,128)(2,1)S(1)} %copy-done.1), kind=kOutput, calls=%fused_computation.8 | convolution fusion | flops 805830656 | bytes 4325376 | tf_op jit(solution)/shard_map/dot_general | solution.py:417
  129.7 0.7 copy.15
  130.3 0.7 copy.16
Async XLA Ops:
  0.6 1.2 copy-start
  1.9 1.2 copy-start.2
  3.1 0.9 copy-start.4
  4.0 0.9 copy-start.5
  94.8 21.3 %copy-start.1 = (bf16[2048,256]{1,0:T(8,128)(2,1)S(1)}, bf16[2048,256]{1,0:T(8,128)(2,1)}, u32[]{:S(2)}) copy-start(bf16[2048,256]{1,0:T(8,128)(2,1)} %fac_hbm.1) | copy-start | bytes 3145732
  116.1 11.1 %copy-start.3 = (f32[128,2048]{1,0:T(8,128)S(1)}, f32[128,2048]{1,0:T(8,128)}, u32[]{:S(2)}) copy-start(f32[128,2048]{1,0:T(8,128)} %old.1) | copy-start | bytes 3145732
